TPU v7x, 32 devices: a whole 2x2x4 slice. The times are simulated.
32 devices in a mesh: grp: 2 (over y), fs: 8 (over z, core), tp: 2 (over x).
Axes of the slice: x: 2, y: 2, z: 4, core: 2. Of those that a mesh axis runs over, the one named last changes fastest.
Arguments:
- prompt: bfloat16 [6144, 2048], P(('grp', 'fs')), parts along dimension 0, may hold values from -6 to 6
- routes: int32 [6144, 4], P(('grp', 'fs')), parts along dimension 0, may hold values from 0 to 7, all different within a row; in each aligned block of 384 rows (0 to 383, 384 to 767, ...) at most 240 rows name the same one
- route_weight: float32 [6144, 4], P(('grp', 'fs')), parts along dimension 0, may hold values from 0.2 to 1
- norm_gain: float32 [2048], P('fs'), may hold values from 0.1 to 1.9
- gate_train: float32 [8, 2048, 1024], P(None, 'fs', 'tp'), may hold values from -0.4 to 0.4
- up_train: float32 [8, 2048, 1024], P(None, 'fs', 'tp'), may hold values from -0.4 to 0.4
- down_train: float32 [8, 1024, 2048], P(None, 'fs', 'tp'), may hold values from -0.07 to 0.07
Outputs:
- gate_serve: bfloat16 [16, 2048, 1024], P(('grp', 'fs'), None, 'tp'), parts along dimension 0
- up_serve: bfloat16 [16, 2048, 1024], P(('grp', 'fs'), None, 'tp'), parts along dimension 0
- down_serve: bfloat16 [16, 1024, 2048], P(('grp', 'fs'), 'tp'), parts along dimension 0
- mixed: bfloat16 [6144, 2048], P(('grp', 'fs'), 'tp'), parts along dimension 0
There are 2 independent parts, one for each index of `grp`. A program takes and returns all parts, laid end to end along the dimension named above; an argument that names none is the same for every part. Nothing has to cross between parts.
Inputs may be any that keep to these rules, and one draw needn't show every extreme that they name: `routes`: each row names 4 different experts. Among the rows of one index of fs no expert is named more than 240 times, a bound that some block reaches on some index.
All inputs are finite; a program needn't handle non-finite values.
Results may differ from a plain program's by a relative error of at most 0.012.
Values may be sent and summed in bfloat16 or wider, within the bound.
No kernel may reach another device: no remote copies, remote signals or barrier semaphores. Data moves between devices by JAX's collectives and lax.ppermute only.
A program may use at most 128 MiB of HBM per device.

v0:
```python
import jax
import jax.numpy as jnp
from jax import lax
from jax.sharding import PartitionSpec as P

TOP = 4


LIMIT = 7.0
ALPHA = 1.702
EPS = 1e-06


def shards(prompt, routes, route_weight, norm_gain, gate_train, up_train, down_train):
    gate_cast = (norm_gain[None, :, None] * gate_train).astype(jnp.bfloat16)
    up_cast = (norm_gain[None, :, None] * up_train).astype(jnp.bfloat16)
    down_cast = down_train.astype(jnp.bfloat16)
    gate_mine, up_mine = (
        lax.all_to_all(gate_cast, "fs", split_axis=0, concat_axis=1, tiled=True),
        lax.all_to_all(up_cast, "fs", split_axis=0, concat_axis=1, tiled=True),
    )
    down_rows = lax.all_to_all(down_cast, "fs", split_axis=0, concat_axis=1, tiled=True)
    down_mine = lax.all_to_all(down_rows, "tp", split_axis=1, concat_axis=2, tiled=True)
    tok_rows, width = prompt.shape
    experts = gate_train.shape[0]
    quarter = width // lax.axis_size("tp")
    capacity = min(tok_rows, max(2, 5 * tok_rows * TOP // (4 * experts)))
    values = prompt.astype(jnp.float32)
    normed = (values * lax.rsqrt(jnp.mean(values * values, axis=-1, keepdims=True) + EPS)).astype(
        jnp.bfloat16
    )
    flat_expert = routes.reshape(-1)
    onehot = (flat_expert[:, None] == jnp.arange(experts, dtype=jnp.int32)[None, :]).astype(
        jnp.int32
    )
    earlier = jnp.cumsum(onehot, axis=0) - onehot
    slot_pos = jnp.sum(earlier * onehot, axis=1)
    target = flat_expert * capacity + slot_pos
    source_row = jnp.arange(tok_rows * TOP, dtype=jnp.int32) // TOP
    outbox = jnp.zeros((experts * capacity, width), jnp.bfloat16).at[target].set(normed[source_row])
    inbox = lax.all_to_all(
        outbox.reshape(experts, capacity, width), "fs", split_axis=0, concat_axis=1, tiled=True
    )
    gate_pre = jnp.einsum("erd,edf->erf", inbox, gate_mine, preferred_element_type=jnp.float32)
    up_pre = jnp.einsum("erd,edf->erf", inbox, up_mine, preferred_element_type=jnp.float32)
    gate_pre = jnp.minimum(gate_pre, LIMIT)
    up_pre = jnp.clip(up_pre, -LIMIT, LIMIT)
    hidden = ((up_pre + 1.0) * gate_pre * jax.nn.sigmoid(ALPHA * gate_pre)).astype(jnp.bfloat16)
    own_width = hidden.shape[2]
    empty = jnp.zeros((hidden.shape[0], hidden.shape[1], down_rows.shape[2]), jnp.float32)
    total = empty
    piece = lax.all_gather(hidden, "tp", axis=2, tiled=True)
    for index in range(piece.shape[2] // own_width):
        cols = piece[:, :, index * own_width : (index + 1) * own_width]
        weight_rows = lax.dynamic_slice_in_dim(down_rows, index * own_width, own_width, 1)
        part = jnp.einsum(
            "erf,efd->erd", cols, weight_rows, preferred_element_type=jnp.float32
        ).astype(jnp.bfloat16)
        total = total + part.astype(jnp.float32)
    summed = total.astype(jnp.bfloat16)
    back = lax.all_to_all(summed, "fs", split_axis=1, concat_axis=0, tiled=True)
    picked = back.reshape(experts * capacity, quarter)[target].astype(jnp.float32)
    weighted = picked.reshape(tok_rows, TOP, quarter) * route_weight[:, :, None]
    mixed = jnp.sum(weighted, axis=1).astype(jnp.bfloat16)
    return (gate_mine, up_mine, down_mine, mixed)


def solution(mesh):
    return jax.shard_map(
        shards,
        mesh=mesh,
        in_specs=(
            P(("grp", "fs"), None),
            P(("grp", "fs"), None),
            P(("grp", "fs"), None),
            P("fs"),
            P(None, "fs", "tp"),
            P(None, "fs", "tp"),
            P(None, "fs", "tp"),
        ),
        out_specs=(
            P(("grp", "fs"), None, "tp"),
            P(("grp", "fs"), None, "tp"),
            P(("grp", "fs"), "tp", None),
            P(("grp", "fs"), "tp"),
        ),
        check_vma=False,
    )
```

profile of v0, /device:TPU:0, one launch (start us, length us, event | category | flops | bytes accessed | tf_op | source)
XLA Modules:
  0.0 601.1 jit_solution(9907944391653193153)
XLA Ops:
  7.2 6.8 %multiply_convert_fusion = (bf16[8,256,512]{2,1,0:T(8,128)(2,1)}, bf16[8,256,512]{2,1,0:T(8,128)(2,1)}) fusion(f32[8,256,512]{2,1,0:T(8,128)} %param.12, f32[256]{0:T(256)} %param.10, f32[8,256,512]{2,1,0:T(8,128)} %param.11), kind=kLoop, calls=%fused_computation.7 | loop fusion | flops 4194304 | bytes 12583936 | tf_op jit(solution)/shard_map/convert_element_type | solution.py:16
  14.0 0.0 copy-start.4
  14.0 6.5 %all-to-all-start = ((bf16[8,256,512]{2,1,0:T(8,128)(2,1)}), bf16[8,256,512]{2,1,0:T(8,128)(2,1)S(1)}, u32[]{:S(2)}, u32[]{:S(2)}) async-start(bf16[8,256,512]{2,1,0:T(8,128)(2,1)} %get-tuple-element.17), calls=%async_computation | async-start | bytes 4194304 | tf_op jit(solution)/shard_map/all_to_all | solution.py:19
  20.5 0.0 copy-done.4
  20.5 0.1 copy.32
  20.6 0.1 eq.29
  20.8 0.1 eq.25
  20.9 2.3 reduce-window.6
  23.2 0.3 slice_reduce_fusion
  23.5 0.2 reduce-window.9
  23.7 0.1 copy.31
  23.8 0.2 mul.72
  24.0 0.3 fusion.12
  24.3 0.1 add_bitcast_fusion
  24.5 1.8 fusion.4
  26.3 2.9 fusion.5
  29.2 33.3 %scatter_custom_fusion = bf16[1920,2048]{1,0:T(8,128)(2,1)} fusion(s32[1536]{0:T(1024)S(1)} %fusion.11, bf16[384,2048]{1,0:T(8,128)(2,1)} %fusion.5, s32[2048]{0:T(1024)S(1)} %pad_clamp_fusion.1, bf16[]{:T(256)} %constant.17.clone.1), kind=kCustom, calls=%fused_computation.4 | custom fusion | bytes 7864832 | tf_op jit(solution)/shard_map/scatter | solution.py:40
  62.5 7.0 %all-to-all-done = bf16[8,256,512]{2,1,0:T(8,128)(2,1)S(1)} async-done(((bf16[8,256,512]{2,1,0:T(8,128)(2,1)}), bf16[8,256,512]{2,1,0:T(8,128)(2,1)S(1)}, u32[]{:S(2)}, u32[]{:S(2)}) %all-to-all-start) | async-done | bytes 2097184 | tf_op jit(solution)/shard_map/all_to_all | solution.py:19
  69.5 0.0 copy-start.2
  69.5 178.2 %all_to_all.72 = bf16[8,240,2048]{2,1,0:T(8,128)(2,1)} all-to-all(bf16[8,240,2048]{2,1,0:T(8,128)(2,1)} %bitcast.61), channel_id=1, replica_groups=mesh['grp'=2,'fs'=8,'tp'=2] {'fs'}, dimensions={0} | all-to-all | bytes 15728640 | tf_op jit(solution)/shard_map/all_to_all | solution.py:41
  247.7 4.4 all-to-all-start.1
  252.1 0.0 all-gather.3.cloned.1.call-start
  252.1 0.0 copy-done.2
  252.1 9.5 %fusion.13 = f32[1920,512]{1,0:T(8,128)} fusion(bf16[1920,2048]{1,0:T(8,128)(2,1)} %bitcast.73, bf16[2048,512]{1,0:T(8,128)(2,1)S(1)} %bitcast.70), kind=kOutput, calls=%fused_computation.45 | convolution fusion | flops 4026531840 | bytes 13893632 | tf_op jit(solution)/shard_map/erd,edf->erf/dot_general | solution.py:44
  261.6 39.5 %all-to-all-done.1 = bf16[8,256,512]{2,1,0:T(8,128)(2,1)} async-done(((bf16[8,256,512]{2,1,0:T(8,128)(2,1)}), bf16[8,256,512]{2,1,0:T(8,128)(2,1)}, u32[]{:S(2)}, u32[]{:S(2)}) %all-to-all-start.1) | async-done | bytes 2097184 | tf_op jit(solution)/shard_map/all_to_all | solution.py:20
  301.1 11.8 %multiply_convert_fusion.2 = bf16[1920,512]{1,0:T(8,128)(2,1)} fusion(f32[1920,512]{1,0:T(8,128)} %fusion.13, bf16[1920,2048]{1,0:T(8,128)(2,1)} %bitcast.74, bf16[2048,512]{1,0:T(8,128)(2,1)} %bitcast.8), kind=kOutput, calls=%fused_computation.11 | convolution fusion | flops 4036362240 | bytes 15859712 | tf_op jit(solution)/shard_map/erd,edf->erf/dot_general | solution.py:45
  312.9 0.0 all-gather.3.cloned.1.call-update
  312.9 2.5 convert_element_type.62
  315.4 51.6 %all_to_all.73 = bf16[8,128,1024]{2,1,0:T(8,128)(2,1)S(1)} all-to-all(bf16[8,128,1024]{2,1,0:T(8,128)(2,1)S(1)} %convert_element_type.62), channel_id=1, replica_groups=mesh['grp'=2,'fs'=8,'tp'=2] {'fs'}, dimensions={0} | all-to-all | bytes 4194304 | tf_op jit(solution)/shard_map/all_to_all | solution.py:22
  367.1 0.0 copy-start
  367.1 1.3 copy-done
  368.4 5.2 copy.46
  373.5 0.5 broadcast.146
  374.1 12.8 %reduce.6 = bf16[1024,1024]{1,0:T(8,128)(2,1)S(1)} reduce(bf16[1024,1,1024]{2,1,0:T(2,128)(2,1)} %bitcast.64, bf16[]{:T(256)} %broadcast.146), dimensions={1}, to_apply=%bitcast.58.reduce_sub_computation | reduce | bytes 4194306
  386.8 2.5 reshape.227
  389.4 4.0 all-to-all-start.3
  393.3 0.0 all-gather.3.cloned.1.call-done
  393.4 0.0 copy-start.1
  393.4 0.0 copy-start.6
  393.4 4.2 fusion.6
  397.6 0.0 copy-done.1
  397.6 0.0 copy-done.6
  397.6 2.3 fusion.2
  399.9 27.0 %copy.45 = bf16[1,1920,1024]{2,0,1:T(2,128)(2,1)} copy(bf16[1,1920,1024]{2,1,0:T(8,128)(2,1)S(1)} %fusion.2) | data formatting | bytes 7864320 | tf_op jit(solution)/shard_map/convert_element_type | solution.py:60
  426.8 24.6 %reduce.7 = bf16[1920,1024]{1,0:T(8,128)(2,1)} reduce(bf16[1920,1,1024]{2,1,0:T(2,128)(2,1)} %bitcast.62, bf16[]{:T(256)} %broadcast.146), dimensions={1}, to_apply=%bitcast.57.reduce_sub_computation | reduce | bytes 7864322
  451.4 7.6 %reshape.225 = bf16[8,2,122880]{2,1,0:T(2,128)(2,1)} reshape(bf16[1920,1024]{1,0:T(8,128)(2,1)} %reduce.7) | data formatting | bytes 7864320
  459.1 0.0 copy-start.5
  459.1 0.0 all-to-all-done.3
  459.1 4.9 all-to-all-start.5
  464.0 0.0 copy-done.5
  464.0 0.1 copy.35
  464.2 3.1 reshape.228
  467.3 3.0 copy.37
  470.3 2.6 copy.30
  472.8 3.9 copy.36
  476.7 75.6 %all-to-all-done.5 = bf16[8,2,122880]{2,1,0:T(2,128)(2,1)} async-done(((bf16[8,2,122880]{2,1,0:T(2,128)(2,1)}), bf16[8,2,122880]{2,1,0:T(2,128)(2,1)}, u32[]{:S(2)}, u32[]{:S(2)}) %all-to-all-start.5) | async-done | bytes 3932192 | tf_op jit(solution)/shard_map/all_to_all | solution.py:61
  552.4 8.5 %reshape.226 = bf16[1920,1,1024]{2,1,0:T(2,128)(2,1)} reshape(bf16[8,2,122880]{2,1,0:T(2,128)(2,1)} %all-to-all-done.5) | data formatting | bytes 7864320
  560.8 6.8 %copy.44 = bf16[1,1920,1024]{2,1,0:T(8,128)(2,1)} copy(bf16[1,1920,1024]{2,0,1:T(2,128)(2,1)} %bitcast.63) | data formatting | bytes 7864320
  567.7 9.7 %gather_fusion = bf16[1536,1024]{1,0:T(8,128)(2,1)S(1)} fusion(bf16[1920,1024]{1,0:T(8,128)(2,1)} %bitcast.60, s32[2048]{0:T(1024)S(1)} %pad_clamp_fusion), kind=kCustom, calls=%fused_computation.1 | custom fusion | bytes 6297600 | tf_op jit(solution)/shard_map/gather | solution.py:62
  577.4 4.4 reshape.190
  581.8 7.9 %multiply_reduce_fusion = bf16[384,1024]{1,0:T(8,128)(2,1)} fusion(f32[384,4,1024]{2,1,0:T(4,128)} %reshape.190, f32[384,4]{1,0:T(8,128)S(1)} %copy.35), kind=kLoop, calls=%fused_computation.6 | loop fusion | flops 2752512 | bytes 7084032 | tf_op jit(solution)/shard_map/reduce_sum | solution.py:64
  589.6 0.0 copy-done.3
  589.6 1.3 copy.49
  591.0 3.0 copy.50
  (8 shorter events, 0.1 us)
Async XLA Ops:
  14.0 6.5 %copy-start.4 = (s32[384,4]{0,1:T(4,128)S(1)}, s32[384,4]{0,1:T(4,128)}, u32[]{:S(2)}) copy-start(s32[384,4]{0,1:T(4,128)} %param.8) | copy-start | bytes 18436
  14.0 55.5 %all-to-all-start = ((bf16[8,256,512]{2,1,0:T(8,128)(2,1)}), bf16[8,256,512]{2,1,0:T(8,128)(2,1)S(1)}, u32[]{:S(2)}, u32[]{:S(2)}) async-start(bf16[8,256,512]{2,1,0:T(8,128)(2,1)} %get-tuple-element.17), calls=%async_computation | async-start | bytes 4194304 | tf_op jit(solution)/shard_map/all_to_all | solution.py:19
  69.5 182.6 %copy-start.2 = (bf16[8,256,512]{2,1,0:T(8,128)(2,1)}, bf16[8,256,512]{2,1,0:T(8,128)(2,1)S(1)}, u32[]{:S(2)}) copy-start(bf16[8,256,512]{2,1,0:T(8,128)(2,1)S(1)} %all-to-all-done) | copy-start | bytes 6291460
  247.7 53.4 %all-to-all-start.1 = ((bf16[8,256,512]{2,1,0:T(8,128)(2,1)}), bf16[8,256,512]{2,1,0:T(8,128)(2,1)}, u32[]{:S(2)}, u32[]{:S(2)}) async-start(bf16[8,256,512]{2,1,0:T(8,128)(2,1)} %get-tuple-element.16), calls=%async_computation.1 | async-start | bytes 4194304 | tf_op jit(solution)/shard_map/all_to_all | solution.py:20
  252.1 141.3 %all-gather.3.cloned.1.call-start = ((), (), s32[]{:S(2)}) async-start(), calls=%async_computation.6 | async-start | bytes 5898240 | tf_op jit(solution)/shard_map/all_gather | solution.py:52
  367.1 1.3 copy-start
  389.4 69.7 %all-to-all-start.3 = ((bf16[2,2,262144]{2,1,0:T(2,128)(2,1)}), bf16[2,2,262144]{2,1,0:T(2,128)(2,1)S(1)}, u32[]{:S(2)}, u32[]{:S(2)}) async-start(bf16[2,2,262144]{2,1,0:T(2,128)(2,1)} %reshape.227), calls=%async_computation.3 | async-start | bytes 4194304 | tf_op jit(solution)/shard_map/all_to_all | solution.py:23
  393.4 4.2 copy-start.1
  393.4 4.2 copy-start.6
  459.1 4.9 copy-start.5
  459.1 93.3 %all-to-all-start.5 = ((bf16[8,2,122880]{2,1,0:T(2,128)(2,1)}), bf16[8,2,122880]{2,1,0:T(2,128)(2,1)}, u32[]{:S(2)}, u32[]{:S(2)}) async-start(bf16[8,2,122880]{2,1,0:T(2,128)(2,1)} %reshape.225), calls=%async_computation.5 | async-start | bytes 7864320 | tf_op jit(solution)/shard_map/all_to_all | solution.py:61
  581.8 7.9 %copy-start.3 = (bf16[8,256,512]{2,1,0:T(8,128)(2,1)S(1)}, bf16[8,256,512]{2,1,0:T(8,128)(2,1)}, u32[]{:S(2)}) copy-start(bf16[8,256,512]{2,1,0:T(8,128)(2,1)} %copy-done.2) | copy-start | bytes 6291460
Sparse Core Ops, SparseCore 0:
  313.0 52.6 all-gather.2
where the time goes:
time: 605 us; the launch traced here: 601 us
  blocking collectives  230 us (38%)
  local copies, waits for them, and re-layouts  125 us (21%)
  waiting for transfers between devices  122 us (20%)
  other arithmetic  62.2 us (10%)
  matrix products  27.7 us (5%)
  starting transfers between devices  19.8 us (3%)
  between operations  14.5 us (2%)
    all_to_all x1, blocking collectives, shards(): lax.all_to_all(outbox.reshape(experts, capacity, width), 'fs', split_axis...  178 us
    all_to_all x1, waiting for transfers between devices, shards(): back = lax.all_to_all(summed, 'fs', split_axis=1, concat_axis=0, tiled=True)  75.6 us
    all_to_all x1, blocking collectives, shards(): lax.all_to_all(down_cast, 'fs', split_axis=0, concat_axis=1, tiled=True)  51.6 us
    unnamed x26, local copies, waits for them, and re-layouts  41.9 us
    all_to_all x1, waiting for transfers between devices, shards(): lax.all_to_all(up_cast, 'fs', split_axis=0, concat_axis=1, tiled=True)  39.5 us
    unnamed x3, other arithmetic  37.4 us
    scatter x1, local copies, waits for them, and re-layouts, shards(): jnp.zeros((experts * capacity, width), jnp.bfloat16).at[target]  33.3 us
    convert_element_type x1, local copies, waits for them, and re-layouts, shards(): summed = total.astype(jnp.bfloat16)  27 us
  transfers between devices with their start and end apart: 5, of which 3 were waited for; matrix products, arithmetic and copies ran while one was open for 26% of the time, Pallas kernels for 0%

commit v1 on v0

v1 whole, which is shorter than its diff:
```python
import jax
import jax.numpy as jnp
from jax import lax
from jax.sharding import PartitionSpec as P

LIMIT = 7.0
ALPHA = 1.702
EPS = 1e-06


def ring_pieces(send_block, axis):
    size = lax.axis_size(axis)
    pieces = [send_block(0)]
    for step in range(1, size):
        perm = [(src, (src + step) % size) for src in range(size)]
        pieces.append(lax.ppermute(send_block(step), axis, perm))
    return pieces


def by_source(pieces, axis):
    size = len(pieces)
    me = lax.axis_index(axis)
    ordered = []
    for source in range(size):
        step = (me - source) % size
        out = pieces[0]
        for index in range(1, size):
            out = jnp.where(step == index, pieces[index], out)
        ordered.append(out)
    return ordered


def shards(prompt, routes, route_weight, norm_gain, gate_train, up_train, down_train):
    grp, fs, tp = (lax.axis_size(name) for name in ("grp", "fs", "tp"))
    my_grp, my_tp = lax.axis_index("grp"), lax.axis_index("tp")
    tok_rows, width = prompt.shape
    top = routes.shape[1]
    experts, d_rows, own_width = gate_train.shape
    f_rows, out_cols = down_train.shape[1:]
    capacity = min(tok_rows, max(2, 5 * tok_rows * top // (4 * experts)))

    chosen = routes[None, :, :] == jnp.arange(experts, dtype=jnp.int32)[:, None, None]
    table = jnp.sum(jnp.where(chosen, route_weight[None, :, :], 0.0), axis=2)
    weight = lax.all_to_all(table, "fs", split_axis=0, concat_axis=0, tiled=True)
    values = prompt.astype(jnp.float32)
    normed = (values * lax.rsqrt(jnp.mean(values * values, axis=-1, keepdims=True) + EPS)).astype(
        jnp.bfloat16
    )
    tokens = lax.all_gather(normed, "fs", axis=0, tiled=False)

    share = d_rows // grp
    gain = norm_gain[None, :, None]
    start = my_grp * share
    gate_part = lax.dynamic_slice_in_dim(gate_train, start, share, 1)
    up_part = lax.dynamic_slice_in_dim(up_train, start, share, 1)
    gain_part = lax.dynamic_slice_in_dim(gain, start, share, 1)
    both = jnp.concatenate([gain_part * gate_part, gain_part * up_part], axis=1).astype(jnp.bfloat16)
    both = lax.all_to_all(both, "fs", split_axis=0, concat_axis=0, tiled=True)
    both = by_source(ring_pieces(lambda step: both, "grp"), "grp")
    gate_mine, up_mine = (
        jnp.stack([piece[:, at : at + share] for piece in both], axis=1).reshape(
            fs * d_rows, own_width
        )
        for at in (0, share)
    )
    f_share = f_rows // grp
    down_part = lax.dynamic_slice_in_dim(down_train, my_grp * f_share, f_share, 1).astype(
        jnp.bfloat16
    )
    down_part = lax.all_to_all(down_part, "fs", split_axis=0, concat_axis=0, tiled=True)
    down_part = by_source(ring_pieces(lambda step: down_part, "grp"), "grp")
    down_rows = jnp.stack(down_part, axis=1).reshape(fs * f_rows, out_cols)

    def down_block(step):
        return lax.dynamic_slice_in_dim(
            down_rows, ((my_tp + step) % tp) * own_width, own_width, 0
        )

    down_mine = jnp.concatenate(by_source(ring_pieces(down_block, "tp"), "tp"), axis=1)

    mask = weight > 0.0
    flags = mask.astype(jnp.bfloat16)
    order = jnp.arange(tok_rows, dtype=jnp.int32)
    before = (order[:, None] < order[None, :]).astype(jnp.bfloat16)
    place = jnp.dot(flags, before, preferred_element_type=jnp.float32).astype(jnp.int32)
    slots = jnp.arange(capacity, dtype=jnp.int32)
    pick = ((place[:, None, :] == slots[None, :, None]) & mask[:, None, :]).astype(jnp.bfloat16)
    inbox = (
        jnp.einsum("sct,std->scd", pick, tokens, preferred_element_type=jnp.float32)
        .astype(jnp.bfloat16)
        .reshape(fs * capacity, width)
    )
    gate_pre = jnp.dot(inbox, gate_mine, preferred_element_type=jnp.float32)
    up_pre = jnp.dot(inbox, up_mine, preferred_element_type=jnp.float32)
    gate_pre = jnp.minimum(gate_pre, LIMIT)
    up_pre = jnp.clip(up_pre, -LIMIT, LIMIT)
    hidden = ((up_pre + 1.0) * gate_pre * jax.nn.sigmoid(ALPHA * gate_pre)).astype(jnp.bfloat16)
    total = 0.0
    for step, cols in enumerate(ring_pieces(lambda step: hidden, "tp")):
        total = total + jnp.dot(cols, down_block(-step), preferred_element_type=jnp.float32)
    summed = total.astype(jnp.bfloat16).reshape(fs, capacity, out_cols)
    back = jnp.einsum("sct,scd->std", pick, summed, preferred_element_type=jnp.float32)
    back = (back * weight[:, :, None]).astype(jnp.bfloat16).reshape(fs * tok_rows, out_cols)
    mixed = lax.psum_scatter(back, "fs", scatter_dimension=0, tiled=True)
    return (gate_mine[None], up_mine[None], down_mine[None], mixed)


def solution(mesh):
    return jax.shard_map(
        shards,
        mesh=mesh,
        in_specs=(
            P(("grp", "fs"), None),
            P(("grp", "fs"), None),
            P(("grp", "fs"), None),
            P("fs"),
            P(None, "fs", "tp"),
            P(None, "fs", "tp"),
            P(None, "fs", "tp"),
        ),
        out_specs=(
            P(("grp", "fs"), None, "tp"),
            P(("grp", "fs"), None, "tp"),
            P(("grp", "fs"), "tp", None),
            P(("grp", "fs"), "tp"),
        ),
        check_vma=False,
    )
```

time: 605 us -> 345 us (0.57)
  blocking collectives: 230 us -> 110 us
  local copies, waits for them, and re-layouts: 125 us -> 5.15 us
  other arithmetic: 62.2 us -> 15 us
  waiting for transfers between devices: 122 us -> 154 us
    all_to_all x2 -> x1, blocking collectives: 230 us -> 110 us  [shards(): both = lax.all_to_all(both, 'fs', split_axis=0, concat_axis=0, tiled=True)]
    all_to_all x4 -> x2, waiting for transfers between devices: 122 us -> 47.5 us  [the longest x1 44.5 us: shards(): lax.all_to_all(down_part, 'fs', split_axis=0, concat_axis=0, tiled=True)]
    ppermute x0 -> x4, waiting for transfers between devices: none -> 61.4 us  [ring_pieces(): pieces.append(lax.ppermute(send_block(step), axis, perm))]
    unnamed x26 -> x11, local copies, waits for them, and re-layouts: 41.9 us -> 0.03 us
    reduce_scatter x0 -> x1, waiting for transfers between devices: none -> 41 us  [shards(): mixed = lax.psum_scatter(back, 'fs', scatter_dimension=0, tiled=True)]
    unnamed x3 -> x0, other arithmetic: 37.4 us -> none
    scatter x1 -> x0, local copies, waits for them, and re-layouts: 33.3 us -> none  [shards(): jnp.zeros((experts * capacity, width), jnp.bfloat16).at[target]]
    convert_element_type x2 -> x1, local copies, waits for them, and re-layouts: 31.3 us -> 2.74 us  [shards(): lax.dynamic_slice_in_dim(down_train, my_grp * f_share, f_share, 1)]
  transfers between devices with their start and end apart: 5 -> 8, of which waited for: 3 -> 6; matrix products, arithmetic and copies ran while one was open for 26% -> 11% of each run, Pallas kernels for 0% -> 0%
where the time goes in v1:
time: 345 us
  waiting for transfers between devices  154 us (45%)
  blocking collectives  110 us (32%)
  matrix products  32 us (9%)
  other arithmetic  15 us (4%)
  starting transfers between devices  14.8 us (4%)
  between operations  14.3 us (4%)
  local copies, waits for them, and re-layouts  5.15 us (1%)
    all_to_all x1, blocking collectives, shards(): both = lax.all_to_all(both, 'fs', split_axis=0, concat_axis=0, tiled=True)  110 us
    ppermute x4, waiting for transfers between devices, ring_pieces(): pieces.append(lax.ppermute(send_block(step), axis, perm))  61.4 us
    all_to_all x1, waiting for transfers between devices, shards(): lax.all_to_all(down_part, 'fs', split_axis=0, concat_axis=0, tiled=True)  44.5 us
    reduce_scatter x1, waiting for transfers between devices, shards(): mixed = lax.psum_scatter(back, 'fs', scatter_dimension=0, tiled=True)  41 us
    dot_general x1, matrix products, shards(): jnp.einsum('sct,std->scd', pick, tokens, preferred_element_type=jnp.float32)  9.29 us
    dot_general x2, matrix products, shards(): jnp.dot(cols, down_block(-step), preferred_element_type=jnp.float32)  7.78 us
  transfers between devices with their start and end apart: 8, of which 6 were waited for; matrix products, arithmetic and copies ran while one was open for 11% of the time, Pallas kernels for 0%

profile of v1, /device:TPU:0, one launch (start us, length us, event | category | flops | bytes accessed | tf_op | source)
XLA Modules:
  0.0 344.9 jit_solution(3906362324578496916)
XLA Ops:
  7.2 0.0 copy-start.4
  7.2 0.0 all-gather.3.cloned.1.call-start
  7.2 1.8 fusion
  9.0 2.9 fusion.1
  11.9 0.0 all-gather.3.cloned.1.call-update
  11.9 0.0 copy-done.4
  11.9 0.1 dynamic_slice.22
  12.0 2.9 multiply_convert_fusion.3
  14.9 0.1 pad_maximum_fusion
  15.1 0.0 copy-start.2
  15.1 0.0 copy-start.3
  15.1 110.2 %all_to_all.22 = bf16[8,256,512]{2,1,0:T(8,128)(2,1)S(1)} all-to-all(bf16[8,256,512]{2,1,0:T(8,128)(2,1)S(1)} %pad_maximum_fusion), channel_id=1, replica_groups=mesh['grp'=2,'fs'=8,'tp'=2] {'fs'}, dimensions={0} | all-to-all | bytes 4194304 | tf_op jit(solution)/shard_map/all_to_all | solution.py:58
  125.3 1.5 collective-permute-start
  126.8 0.0 copy-done.2
  126.8 0.0 copy-done.3
  126.8 0.6 copy.48
  127.5 3.3 all-to-all-start.2
  130.8 2.7 dynamic-slice_convert_fusion
  133.5 3.1 all-to-all-done.2
  136.6 5.7 %all-to-all-start.1 = ((bf16[8,64,1024]{2,1,0:T(8,128)(2,1)}), bf16[8,64,1024]{2,1,0:T(8,128)(2,1)S(1)}, u32[]{:S(2)}, u32[]{:S(2)}) async-start(bf16[8,64,1024]{2,1,0:T(8,128)(2,1)} %dynamic-slice_convert_fusion), calls=%async_computation.1 | async-start | bytes 2097152 | tf_op jit(solution)/shard_map/all_to_all | solution.py:70
  142.3 0.0 reduce-scatter.2.cloned.1.call-start
  142.4 0.1 convolution_convert_fusion.1
  142.5 44.5 %all-to-all-done.1 = bf16[8,64,1024]{2,1,0:T(8,128)(2,1)S(1)} async-done(((bf16[8,64,1024]{2,1,0:T(8,128)(2,1)}), bf16[8,64,1024]{2,1,0:T(8,128)(2,1)S(1)}, u32[]{:S(2)}, u32[]{:S(2)}) %all-to-all-start.1) | async-done | bytes 1048608 | tf_op jit(solution)/shard_map/all_to_all | solution.py:70
  187.0 1.2 collective-permute-start.1
  188.1 0.0 collective-permute-done
  188.1 1.9 broadcast_select_fusion.1
  190.0 0.3 slice_bitcast_fusion
  190.3 0.2 pad_maximum_fusion.2
  190.5 0.2 copy.46
  190.7 0.0 copy-start
  190.7 1.6 pad_maximum_fusion.1
  192.3 3.6 %all-gather.3.cloned.1.call-done = bf16[3072,2048]{1,0:T(8,128)(2,1)} async-done(((bf16[384,2048]{1,0:T(8,128)(2,1)}), bf16[3072,2048]{1,0:T(8,128)(2,1)}) %all-gather.3.cloned.1.call-update) | async-done | bytes 12582928 | tf_op jit(solution)/shard_map/all_gather | solution.py:49
  195.9 0.0 copy-start.1
  195.9 9.3 %convolution_convert_fusion = bf16[8,240,2048]{2,1,0:T(8,128)(2,1)S(1)} fusion(bf16[8,384,2048]{2,1,0:T(8,128)(2,1)} %bitcast.42, s32[8,384]{1,0:T(8,128)S(1)} %convolution_convert_fusion.1, pred[8,384]{1,0:T(8,128)(4,1)S(1)} %compare_bitcast_fusion), kind=kOutput, calls=%fused_computation.2 | convolution fusion | flops 3025305600 | bytes 20462592 | tf_op jit(solution)/shard_map/sct,std->scd/dot_general | solution.py:89
  205.2 0.0 copy-done.1
  205.2 4.3 %fusion.17 = f32[1920,512]{1,0:T(8,128)S(1)} fusion(bf16[1920,2048]{1,0:T(8,128)(2,1)S(1)} %bitcast.47, bf16[2048,512]{1,0:T(8,128)(2,1)S(1)} %bitcast.53), kind=kOutput, calls=%fused_computation.48 | convolution fusion | flops 4026531840 | bytes 13893632 | tf_op jit(solution)/shard_map/dot_general | solution.py:93
  209.6 0.0 copy-done
  209.6 6.3 %multiply_convert_fusion.1 = bf16[1920,512]{1,0:T(8,128)(2,1)} fusion(f32[1920,512]{1,0:T(8,128)S(1)} %fusion.17, bf16[1920,2048]{1,0:T(8,128)(2,1)S(1)} %bitcast.48, bf16[2048,512]{1,0:T(8,128)(2,1)S(1)} %bitcast.50), kind=kOutput, calls=%fused_computation.3 | convolution fusion | flops 4036362240 | bytes 15859712 | tf_op jit(solution)/shard_map/dot_general | solution.py:94
  215.9 1.5 collective-permute-start.3
  217.4 0.0 collective-permute-done.1
  217.4 1.4 select_bitcast_fusion.1
  218.7 0.2 pad_maximum_fusion.3
  218.9 0.2 copy.47
  219.1 3.9 %fusion.10 = f32[1920,1024]{1,0:T(8,128)S(1)} fusion(bf16[1920,512]{1,0:T(8,128)(2,1)} %multiply_convert_fusion.1, bf16[1024,1024]{1,0:T(8,128)(2,1)S(1)} %bitcast.43, s32[]{:T(128)S(6)} %select_n.113), kind=kOutput, calls=%fused_computation.34 | convolution fusion | flops 2013265920 | bytes 10878980 | tf_op jit(solution)/shard_map/dot_general | solution.py:100
  223.0 38.2 %collective-permute-done.3 = bf16[1920,512]{1,0:T(8,128)(2,1)} collective-permute-done((bf16[1920,512]{1,0:T(8,128)(2,1)}, bf16[1920,512]{1,0:T(8,128)(2,1)}, u32[]{:S(2)}, u32[]{:S(2)}) %collective-permute-start.3) | collective-permute-done | bytes 1966112 | tf_op jit(solution)/shard_map/ppermute | solution.py:16
  261.2 3.9 %add_convert_fusion = bf16[1920,1024]{1,0:T(8,128)(2,1)S(1)} fusion(f32[1920,1024]{1,0:T(8,128)S(1)} %fusion.10, bf16[1920,512]{1,0:T(8,128)(2,1)} %collective-permute-done.3, bf16[1024,1024]{1,0:T(8,128)(2,1)S(1)} %bitcast.44, s32[]{:T(128)S(6)} %select_n.119), kind=kOutput, calls=%fused_computation.1 | convolution fusion | flops 2017198080 | bytes 14811140 | tf_op jit(solution)/shard_map/dot_general | solution.py:100
  265.1 4.2 %multiply_convert_fusion = bf16[8,384,1024]{2,1,0:T(8,128)(2,1)} fusion(f32[8,384]{1,0:T(8,128)S(1)} %bitcast.55, bf16[8,240,1024]{2,1,0:T(8,128)(2,1)S(1)} %bitcast.56, s32[8,384]{1,0:T(8,128)S(1)} %convolution_convert_fusion.1, pred[8,384]{1,0:T(8,128)(4,1)S(1)} %compare_bitcast_fusion), kind=kOutput, calls=%fused_computation | convolution fusion | flops 1517715456 | bytes 10251264 | tf_op jit(solution)/shard_map/sct,scd->std/dot_general | solution.py:102
  269.3 0.0 reduce-scatter.2.cloned.1.call-update
  269.3 1.0 constant_dynamic-slice_fusion
  270.3 1.5 collective-permute-start.2
  271.8 23.2 %collective-permute-done.2 = bf16[512,1024]{1,0:T(8,128)(2,1)S(1)} collective-permute-done((bf16[512,1024]{1,0:T(8,128)(2,1)}, bf16[512,1024]{1,0:T(8,128)(2,1)S(1)}, u32[]{:S(2)}, u32[]{:S(2)}) %collective-permute-start.2) | collective-permute-done | bytes 1048608 | tf_op jit(solution)/shard_map/ppermute | solution.py:16
  295.0 0.6 broadcast_select_fusion.3
  295.6 1.5 maximum_bitcast_fusion
  297.1 41.0 %reduce-scatter.2.cloned.1.call-done = bf16[384,1024]{1,0:T(8,128)(2,1)} async-done(((bf16[3072,1024]{1,0:T(8,128)(2,1)}), bf16[384,1024]{1,0:T(8,128)(2,1)}) %reduce-scatter.2.cloned.1.call-update) | async-done | bytes 786448 | tf_op jit(solution)/shard_map/reduce_scatter | solution.py:104
  (4 shorter events, 0.0 us)
Async XLA Ops:
  7.2 4.8 %copy-start.4 = (f32[256]{0:T(256)S(1)}, f32[256]{0:T(256)}, u32[]{:S(2)}) copy-start(f32[256]{0:T(256)} %param.10) | copy-start | bytes 3076
  7.2 188.7 %all-gather.3.cloned.1.call-start = ((), (), s32[]{:S(2)}) async-start(), calls=%async_computation.5 | async-start | bytes 14155776 | tf_op jit(solution)/shard_map/all_gather | solution.py:49
  15.1 111.8 %copy-start.2 = (f32[384,4]{0,1:T(4,128)S(1)}, f32[384,4]{0,1:T(4,128)}, u32[]{:S(2)}) copy-start(f32[384,4]{0,1:T(4,128)} %param.9) | copy-start | bytes 18436
  15.1 111.8 %copy-start.3 = (s32[384,4]{0,1:T(4,128)S(1)}, s32[384,4]{0,1:T(4,128)}, u32[]{:S(2)}) copy-start(s32[384,4]{0,1:T(4,128)} %param.8) | copy-start | bytes 18436
  125.3 62.8 %collective-permute-start = (bf16[8,256,512]{2,1,0:T(8,128)(2,1)S(1)}, bf16[8,256,512]{2,1,0:T(8,128)(2,1)}, u32[]{:S(2)}, u32[]{:S(2)}) collective-permute-start(bf16[8,256,512]{2,1,0:T(8,128)(2,1)S(1)} %all_to_all.22), channel_id=1, source_target_pairs={{0,16},{16,0},{1,17},{17,1},{2,18},{18,2},{3,19},{19,3},{4,20},{20... | collective-permute-start | bytes 6291464 | tf_op jit(solution)/shard_map/ppermute | solution.py:16
  127.5 9.2 %all-to-all-start.2 = ((f32[8,1,384]{2,1,0:T(1,128)}), f32[8,1,384]{2,1,0:T(1,128)S(1)}, u32[]{:S(2)}, u32[]{:S(2)}) async-start(f32[8,1,384]{2,1,0:T(1,128)} %copy.48), calls=%async_computation.2 | async-start | bytes 24576 | tf_op jit(solution)/shard_map/all_to_all | solution.py:44
  136.6 50.3 %all-to-all-start.1 = ((bf16[8,64,1024]{2,1,0:T(8,128)(2,1)}), bf16[8,64,1024]{2,1,0:T(8,128)(2,1)S(1)}, u32[]{:S(2)}, u32[]{:S(2)}) async-start(bf16[8,64,1024]{2,1,0:T(8,128)(2,1)} %dynamic-slice_convert_fusion), calls=%async_computation.1 | async-start | bytes 2097152 | tf_op jit(solution)/shard_map/all_to_all | solution.py:70
  142.3 195.8 %reduce-scatter.2.cloned.1.call-start = ((), (), s32[]{:S(2)}) async-start(), calls=%async_computation.4 | async-start | bytes 7077888 | tf_op jit(solution)/shard_map/reduce_scatter | solution.py:104
  187.0 30.4 %collective-permute-start.1 = (bf16[8,64,1024]{2,1,0:T(8,128)(2,1)S(1)}, bf16[8,64,1024]{2,1,0:T(8,128)(2,1)}, u32[]{:S(2)}, u32[]{:S(2)}) collective-permute-start(bf16[8,64,1024]{2,1,0:T(8,128)(2,1)S(1)} %all-to-all-done.1), channel_id=1, source_target_pairs={{0,16},{16,0},{1,17},{17,1},{2,18},{18,2},{3,19},{19,3},{4,20},{20... | collective-permute-start | bytes 3145736 | tf_op jit(solution)/shard_map/ppermute | solution.py:16
  190.7 18.9 %copy-start = (bf16[8,2,128,512]{3,2,1,0:T(8,128)(2,1)}, bf16[8,2,128,512]{3,2,1,0:T(8,128)(2,1)S(1)}, u32[]{:S(2)}) copy-start(bf16[8,2,128,512]{3,2,1,0:T(8,128)(2,1)S(1)} %copy.46) | copy-start | bytes 6291460
  195.9 9.3 %copy-start.1 = (bf16[8,2,128,512]{3,2,1,0:T(8,128)(2,1)S(1)}, bf16[8,2,128,512]{3,2,1,0:T(8,128)(2,1)}, u32[]{:S(2)}) copy-start(bf16[8,2,128,512]{3,2,1,0:T(8,128)(2,1)} %pad_maximum_fusion.1) | copy-start | bytes 6291460
  215.9 45.3 %collective-permute-start.3 = (bf16[1920,512]{1,0:T(8,128)(2,1)}, bf16[1920,512]{1,0:T(8,128)(2,1)}, u32[]{:S(2)}, u32[]{:S(2)}) collective-permute-start(bf16[1920,512]{1,0:T(8,128)(2,1)} %multiply_convert_fusion.1), channel_id=1, source_target_pairs={{0,1},{1,0},{2,3},{3,2},{4,5},{5,4},{6,7},{7,6},{8,9},{9,8},{10,11... | collective-permute-start | bytes 5898248 | tf_op jit(solution)/shard_map/ppermute | solution.py:16
  270.3 24.7 %collective-permute-start.2 = (bf16[512,1024]{1,0:T(8,128)(2,1)}, bf16[512,1024]{1,0:T(8,128)(2,1)S(1)}, u32[]{:S(2)}, u32[]{:S(2)}) collective-permute-start(bf16[512,1024]{1,0:T(8,128)(2,1)} %constant_dynamic-slice_fusion), channel_id=1, source_target_pairs={{0,1},{1,0},{2,3},{3,2},{4,5},{5,4},{6,7},{7,6},{8,9},{9,8},{10,11... | collective-permute-start | bytes 3145736 | tf_op jit(solution)/shard_map/ppermute | solution.py:16
Sparse Core Ops, SparseCore 0:
  12.0 183.8 all-gather.2
  269.4 68.6 reduce-scatter.1

commit v2 on v1

--- a/solution.py
+++ b/solution.py
@@ -6,6 +6,7 @@
 LIMIT = 7.0
 ALPHA = 1.702
 EPS = 1e-06
+CHUNKS = 2
 
 
 def ring_pieces(send_block, axis):
@@ -46,30 +47,40 @@
     normed = (values * lax.rsqrt(jnp.mean(values * values, axis=-1, keepdims=True) + EPS)).astype(
         jnp.bfloat16
     )
-    tokens = lax.all_gather(normed, "fs", axis=0, tiled=False)
+    near = width // 2
+    near_share = near // tp
+    near_tokens = lax.all_gather(
+        lax.dynamic_slice_in_dim(normed, my_tp * near_share, near_share, 1), "fs", axis=0, tiled=False
+    )
 
     share = d_rows // grp
-    gain = norm_gain[None, :, None]
-    start = my_grp * share
-    gate_part = lax.dynamic_slice_in_dim(gate_train, start, share, 1)
-    up_part = lax.dynamic_slice_in_dim(up_train, start, share, 1)
-    gain_part = lax.dynamic_slice_in_dim(gain, start, share, 1)
-    both = jnp.concatenate([gain_part * gate_part, gain_part * up_part], axis=1).astype(jnp.bfloat16)
-    both = lax.all_to_all(both, "fs", split_axis=0, concat_axis=0, tiled=True)
-    both = by_source(ring_pieces(lambda step: both, "grp"), "grp")
-    gate_mine, up_mine = (
-        jnp.stack([piece[:, at : at + share] for piece in both], axis=1).reshape(
-            fs * d_rows, own_width
-        )
-        for at in (0, share)
-    )
+    gain_part = lax.dynamic_slice_in_dim(norm_gain, my_grp * share, share, 0)[None, :, None]
+
+    def served(mine, rows):
+        pieces = by_source(ring_pieces(lambda step: mine, "grp"), "grp")
+        return jnp.stack(pieces, axis=1).reshape(fs * rows, mine.shape[2])
+
+    def scaled(train):
+        part = lax.dynamic_slice_in_dim(train, my_grp * share, share, 1)
+        return (gain_part * part).astype(jnp.bfloat16)
+
+    def over_fs(part):
+        return lax.all_to_all(part, "fs", split_axis=0, concat_axis=0, tiled=True)
+
+    gate_part = over_fs(scaled(gate_train))
+    up_part = scaled(up_train)
+    gate_part, up_part = lax.optimization_barrier((gate_part, up_part))
+    up_part = over_fs(up_part)
+    far, up_part = lax.optimization_barrier((normed[:, near:], up_part))
+    far_tokens = lax.all_gather(far, "fs", axis=0, tiled=False)
+    gate_mine = served(gate_part, d_rows)
+    up_mine = served(up_part, d_rows)
     f_share = f_rows // grp
     down_part = lax.dynamic_slice_in_dim(down_train, my_grp * f_share, f_share, 1).astype(
         jnp.bfloat16
     )
-    down_part = lax.all_to_all(down_part, "fs", split_axis=0, concat_axis=0, tiled=True)
-    down_part = by_source(ring_pieces(lambda step: down_part, "grp"), "grp")
-    down_rows = jnp.stack(down_part, axis=1).reshape(fs * f_rows, out_cols)
+    far_tokens, down_part = lax.optimization_barrier((far_tokens, down_part))
+    down_rows = served(over_fs(down_part), f_rows)
 
     def down_block(step):
         return lax.dynamic_slice_in_dim(
@@ -85,20 +96,38 @@
     place = jnp.dot(flags, before, preferred_element_type=jnp.float32).astype(jnp.int32)
     slots = jnp.arange(capacity, dtype=jnp.int32)
     pick = ((place[:, None, :] == slots[None, :, None]) & mask[:, None, :]).astype(jnp.bfloat16)
-    inbox = (
-        jnp.einsum("sct,std->scd", pick, tokens, preferred_element_type=jnp.float32)
-        .astype(jnp.bfloat16)
-        .reshape(fs * capacity, width)
-    )
-    gate_pre = jnp.dot(inbox, gate_mine, preferred_element_type=jnp.float32)
-    up_pre = jnp.dot(inbox, up_mine, preferred_element_type=jnp.float32)
-    gate_pre = jnp.minimum(gate_pre, LIMIT)
-    up_pre = jnp.clip(up_pre, -LIMIT, LIMIT)
-    hidden = ((up_pre + 1.0) * gate_pre * jax.nn.sigmoid(ALPHA * gate_pre)).astype(jnp.bfloat16)
-    total = 0.0
-    for step, cols in enumerate(ring_pieces(lambda step: hidden, "tp")):
-        total = total + jnp.dot(cols, down_block(-step), preferred_element_type=jnp.float32)
-    summed = total.astype(jnp.bfloat16).reshape(fs, capacity, out_cols)
+
+    def compact(rows, part):
+        picked = jnp.einsum("sct,std->scd", part, rows, preferred_element_type=jnp.float32)
+        return picked.astype(jnp.bfloat16).reshape(-1, rows.shape[2])
+
+    near_rows = compact(near_tokens, pick)
+    near_rows = ring_pieces(lambda step: near_rows, "tp")
+    chunk = fs // CHUNKS
+    outs = []
+    for at in range(0, fs, chunk):
+        rows = slice(at * capacity, (at + chunk) * capacity)
+        far_rows = compact(far_tokens[at : at + chunk], pick[at : at + chunk])
+
+        def project(mine):
+            total = 0.0
+            for step, piece in enumerate(near_rows):
+                first = ((my_tp - step) % tp) * near_share
+                block = lax.dynamic_slice_in_dim(mine, first, near_share, 0)
+                total = total + jnp.dot(piece[rows], block, preferred_element_type=jnp.float32)
+            return total + jnp.dot(far_rows, mine[near:], preferred_element_type=jnp.float32)
+
+        gate_pre = jnp.minimum(project(gate_mine), LIMIT)
+        up_pre = jnp.clip(project(up_mine), -LIMIT, LIMIT)
+        hidden = ((up_pre + 1.0) * gate_pre * jax.nn.sigmoid(ALPHA * gate_pre)).astype(jnp.bfloat16)
+        outs.append(ring_pieces(lambda step: hidden, "tp"))
+    summed = []
+    for pieces in outs:
+        total = 0.0
+        for step, cols in enumerate(pieces):
+            total = total + jnp.dot(cols, down_block(-step), preferred_element_type=jnp.float32)
+        summed.append(total.astype(jnp.bfloat16).reshape(chunk, capacity, out_cols))
+    summed = jnp.concatenate(summed, axis=0)
     back = jnp.einsum("sct,scd->std", pick, summed, preferred_element_type=jnp.float32)
     back = (back * weight[:, :, None]).astype(jnp.bfloat16).reshape(fs * tok_rows, out_cols)
     mixed = lax.psum_scatter(back, "fs", scatter_dimension=0, tiled=True)

time: 345 us -> 331 us (0.959)
  blocking collectives: 110 us -> 56.8 us
  matrix products: 32 us -> 54.5 us
  waiting for transfers between devices: 154 us -> 165 us
  starting transfers between devices: 14.8 us -> 20.7 us
    all_to_all x1, blocking collectives: 110 us -> 56.8 us  [over_fs(): return lax.all_to_all(part, 'fs', split_axis=0, concat_axis=0, tiled=True)]
    dot_general x3 -> x15, matrix products: 19.9 us -> 42 us  [the longest x8 20.8 us: project(): jnp.dot(piece[rows], block, preferred_element_type=jnp.float32)]
    ppermute x4 -> x7, waiting for transfers between devices: 61.4 us -> 82.9 us  [ring_pieces(): pieces.append(lax.ppermute(send_block(step), axis, perm))]
    all_to_all x1 -> x2, waiting for transfers between devices: 44.5 us -> 36.8 us  [over_fs(): return lax.all_to_all(part, 'fs', split_axis=0, concat_axis=0, tiled=True)]
    ppermute x4 -> x7, starting transfers between devices: 5.68 us -> 9.82 us  [ring_pieces(): pieces.append(lax.ppermute(send_block(step), axis, perm))]
    convert_element_type x0 -> x1, other arithmetic: none -> 3.84 us  [scaled(): return (gain_part * part).astype(jnp.bfloat16)]
    all_gather x1 -> x2, waiting for transfers between devices: 3.6 us -> 0.02 us  [the longest x1 0.02 us: shards(): lax.all_gather(lax.dynamic_slice_in_dim(normed, my_tp * near_share, near_...]
    all_to_all x1 -> x2, starting transfers between devices: 5.67 us -> 7.27 us  [over_fs(): return lax.all_to_all(part, 'fs', split_axis=0, concat_axis=0, tiled=True)]
  transfers between devices with their start and end apart: 8 -> 13, of which waited for: 6 -> 9; matrix products, arithmetic and copies ran while one was open for 11% -> 17% of each run, Pallas kernels for 0% -> 0%
where the time goes in v2:
time: 331 us
  waiting for transfers between devices  165 us (50%)
  blocking collectives  56.8 us (17%)
  matrix products  54.5 us (16%)
  starting transfers between devices  20.7 us (6%)
  between operations  14.1 us (4%)
  other arithmetic  11.6 us (4%)
  local copies, waits for them, and re-layouts  8.33 us (3%)
    ppermute x7, waiting for transfers between devices, ring_pieces(): pieces.append(lax.ppermute(send_block(step), axis, perm))  82.9 us
    all_to_all x1, blocking collectives, over_fs(): return lax.all_to_all(part, 'fs', split_axis=0, concat_axis=0, tiled=True)  56.8 us
    reduce_scatter x1, waiting for transfers between devices, shards(): mixed = lax.psum_scatter(back, 'fs', scatter_dimension=0, tiled=True)  42.2 us
    all_to_all x2, waiting for transfers between devices, over_fs(): return lax.all_to_all(part, 'fs', split_axis=0, concat_axis=0, tiled=True)  36.8 us
    dot_general x8, matrix products, project(): jnp.dot(piece[rows], block, preferred_element_type=jnp.float32)  20.8 us
    dot_general x4, matrix products, project(): jnp.dot(far_rows, mine[near:], preferred_element_type=jnp.float32)  11.1 us
    dot_general x3, matrix products, compact(): jnp.einsum('sct,std->scd', part, rows, preferred_element_type=jnp.float32)  10.1 us
    ppermute x7, starting transfers between devices, ring_pieces(): pieces.append(lax.ppermute(send_block(step), axis, perm))  9.82 us
  transfers between devices with their start and end apart: 13, of which 9 were waited for; matrix products, arithmetic and copies ran while one was open for 17% of the time, Pallas kernels for 0%

profile of v2, /device:TPU:0, one launch (start us, length us, event | category | flops | bytes accessed | tf_op | source)
XLA Modules:
  0.0 330.7 jit_solution(14772879619915419706)
XLA Ops:
  7.2 1.9 fusion.3
  9.2 0.3 fusion.4
  9.5 0.8 constant_dynamic-slice_fusion
  10.4 3.8 %multiply_convert_fusion.1 = (bf16[8,128,512]{2,1,0:T(8,128)(2,1)}, bf16[8,128,512]{2,1,0:T(8,128)(2,1)S(1)}) fusion(f32[8,256,512]{2,1,0:T(8,128)} %param.12, s32[]{:T(128)S(6)} %select_n.148, f32[128]{0:T(128)S(1)} %dynamic_slice.43, f32[8,256,512]{2,1,0:T(8,128)} %param.11), kind=kLoop, calls=%fused_computation.26 | loop fusion | flops 2097152 | bytes 6291972 | tf_op jit(solution)/shard_map/convert_element_type | solution.py:65
  14.2 56.8 %all_to_all.27 = bf16[8,128,512]{2,1,0:T(8,128)(2,1)} all-to-all(bf16[8,128,512]{2,1,0:T(8,128)(2,1)S(1)} %get-tuple-element.27), channel_id=1, replica_groups=mesh['grp'=2,'fs'=8,'tp'=2] {'fs'}, dimensions={0} | all-to-all | bytes 2097152 | tf_op jit(solution)/shard_map/all_to_all | solution.py:68
  71.0 3.7 %all-to-all-start.1 = ((bf16[8,128,512]{2,1,0:T(8,128)(2,1)}), bf16[8,128,512]{2,1,0:T(8,128)(2,1)S(1)}, u32[]{:S(2)}, u32[]{:S(2)}) async-start(bf16[8,128,512]{2,1,0:T(8,128)(2,1)} %get-tuple-element.11), calls=%async_computation.1 | async-start | bytes 2097152 | tf_op jit(solution)/shard_map/all_to_all | solution.py:68
  74.8 1.0 slice.66
  75.7 25.5 %all-to-all-done.1 = bf16[8,128,512]{2,1,0:T(8,128)(2,1)S(1)} async-done(((bf16[8,128,512]{2,1,0:T(8,128)(2,1)}), bf16[8,128,512]{2,1,0:T(8,128)(2,1)S(1)}, u32[]{:S(2)}, u32[]{:S(2)}) %all-to-all-start.1) | async-done | bytes 1048608 | tf_op jit(solution)/shard_map/all_to_all | solution.py:68
  101.2 1.6 collective-permute-start
  102.8 0.6 copy.53
  103.5 3.3 %all-to-all-start.3 = ((f32[8,1,384]{2,1,0:T(1,128)}), f32[8,1,384]{2,1,0:T(1,128)S(1)}, u32[]{:S(2)}, u32[]{:S(2)}) async-start(f32[8,1,384]{2,1,0:T(1,128)} %copy.53), calls=%async_computation.3 | async-start | bytes 24576 | tf_op jit(solution)/shard_map/all_to_all | solution.py:45
  106.8 2.9 dynamic-slice_convert_fusion
  109.8 2.7 all-to-all-done.3
  112.5 0.1 convolution_convert_fusion
  112.6 0.6 collective-permute-start.1
  113.2 14.4 %collective-permute-done = bf16[8,128,512]{2,1,0:T(8,128)(2,1)S(1)} collective-permute-done((bf16[8,128,512]{2,1,0:T(8,128)(2,1)}, bf16[8,128,512]{2,1,0:T(8,128)(2,1)S(1)}, u32[]{:S(2)}, u32[]{:S(2)}) %collective-permute-start) | collective-permute-done | bytes 1048608 | tf_op jit(solution)/shard_map/ppermute | solution.py:17
  127.5 0.1 select_bitcast_fusion.5
  127.7 1.1 fusion.37
  128.8 0.2 pad_maximum_fusion
  129.0 3.9 %fusion.25 = bf16[8,240,512]{2,1,0:T(8,128)(2,1)S(1)} fusion(bf16[8,384,512]{2,1,0:T(8,128)(2,1)} %bitcast.89, s32[8,384]{1,0:T(8,128)S(1)} %convolution_convert_fusion, pred[8,384]{1,0:T(8,128)(4,1)S(1)} %compare_bitcast_fusion), kind=kOutput, calls=%fused_computation.32 | convolution fusion | flops 757432320 | bytes 5127168 | tf_op jit(solution)/shard_map/sct,std->scd/dot_general | solution.py:101
  132.9 1.6 collective-permute-start.4
  134.4 14.3 %collective-permute-done.1 = bf16[8,128,512]{2,1,0:T(8,128)(2,1)} collective-permute-done((bf16[8,128,512]{2,1,0:T(8,128)(2,1)S(1)}, bf16[8,128,512]{2,1,0:T(8,128)(2,1)}, u32[]{:S(2)}, u32[]{:S(2)}) %collective-permute-start.1) | collective-permute-done | bytes 1048608 | tf_op jit(solution)/shard_map/ppermute | solution.py:17
  148.7 1.4 select_bitcast_fusion.3
  150.1 0.1 fusion.36
  150.3 0.2 pad_maximum_fusion.1
  150.5 0.2 copy.51
  150.7 0.2 fusion.78
  150.8 2.0 fusion.60
  152.8 2.0 fusion.54
  154.8 0.7 fusion.58
  155.4 3.1 fusion.52
  158.5 16.5 %collective-permute-done.4 = bf16[1920,512]{1,0:T(8,128)(2,1)S(1)} collective-permute-done((bf16[1920,512]{1,0:T(8,128)(2,1)S(1)}, bf16[1920,512]{1,0:T(8,128)(2,1)S(1)}, u32[]{:S(2)}, u32[]{:S(2)}) %collective-permute-start.4) | collective-permute-done | bytes 1966112 | tf_op jit(solution)/shard_map/ppermute | solution.py:17
  175.0 2.0 fusion.44
  177.0 2.0 fusion.41
  179.0 3.1 fusion.15
  182.1 2.5 fusion.79
  184.6 2.4 fusion.80
  187.1 3.6 %all-to-all-start.2 = ((bf16[8,64,1024]{2,1,0:T(8,128)(2,1)}), bf16[8,64,1024]{2,1,0:T(8,128)(2,1)S(1)}, u32[]{:S(2)}, u32[]{:S(2)}) async-start(bf16[8,64,1024]{2,1,0:T(8,128)(2,1)} %dynamic-slice_convert_fusion), calls=%async_computation.2 | async-start | bytes 2097152 | tf_op jit(solution)/shard_map/all_to_all | solution.py:68
  190.6 0.2 reduce-scatter.2.cloned.1.call-start
  190.9 6.7 %multiply_convert_fusion.4 = bf16[960,512]{1,0:T(8,128)(2,1)} fusion(f32[960,512]{1,0:T(8,128)} %fusion.80, f32[960,512]{1,0:T(8,128)} %fusion.54, f32[960,512]{1,0:T(8,128)} %fusion.79, f32[960,512]{1,0:T(8,128)} %fusion.60, f32[960,512]{1,0:T(8,128)} %fusion.44, bf16[1920,512]{1,0:T(8,128)(2,1)} %copy-done.5, bf16[2048,512]{1,0:T(8,128)(2,1)} %bitcast.77, ...), kind=kOutput, calls=%fused_computation.29 | convolution fusion | flops 510197760 | bytes 12320772 | tf_op jit(solution)/shard_map/dot_general | solution.py:117
  197.5 1.5 collective-permute-start.5
  199.0 3.1 fusion.20
  202.2 1.3 copy-done.14
  203.4 2.5 fusion.81
  205.9 11.3 %all-to-all-done.2 = bf16[8,64,1024]{2,1,0:T(8,128)(2,1)S(1)} async-done(((bf16[8,64,1024]{2,1,0:T(8,128)(2,1)}), bf16[8,64,1024]{2,1,0:T(8,128)(2,1)S(1)}, u32[]{:S(2)}, u32[]{:S(2)}) %all-to-all-start.2) | async-done | bytes 1048608 | tf_op jit(solution)/shard_map/all_to_all | solution.py:68
  217.2 1.6 collective-permute-start.2
  218.8 3.7 %fusion.82 = f32[960,512]{1,0:T(8,128)S(1)} fusion(bf16[960,1024]{1,0:T(8,128)(2,1)} %bitcast.91, bf16[1024,512]{1,0:T(8,128)(2,1)} %bitcast.81), kind=kOutput, calls=%fused_computation.104 | convolution fusion | flops 1006632960 | bytes 4980736 | tf_op jit(solution)/shard_map/dot_general | solution.py:118
  222.5 2.5 multiply_convert_fusion.3
  225.1 1.5 collective-permute-start.6
  226.6 15.3 %collective-permute-done.2 = bf16[8,64,1024]{2,1,0:T(8,128)(2,1)S(1)} collective-permute-done((bf16[8,64,1024]{2,1,0:T(8,128)(2,1)S(1)}, bf16[8,64,1024]{2,1,0:T(8,128)(2,1)S(1)}, u32[]{:S(2)}, u32[]{:S(2)}) %collective-permute-start.2) | collective-permute-done | bytes 1048608 | tf_op jit(solution)/shard_map/ppermute | solution.py:17
  241.9 0.1 select_bitcast_fusion.1
  242.0 0.2 pad_maximum_fusion.2
  242.2 0.2 copy.52
  242.4 2.4 fusion.48
  244.8 1.2 fusion.46
  246.0 2.4 add_convert_fusion.1
  248.5 1.2 add_convert_fusion
  249.7 5.1 %multiply_convert_fusion = bf16[8,384,1024]{2,1,0:T(8,128)(2,1)} fusion(f32[8,384]{1,0:T(8,128)S(1)} %bitcast.86, bf16[4,240,1024]{2,1,0:T(8,128)(2,1)S(1)} %bitcast.93, bf16[4,240,1024]{2,1,0:T(8,128)(2,1)S(1)} %bitcast.92, s32[8,384]{1,0:T(8,128)S(1)} %convolution_convert_fusion, pred[8,384]{1,0:T(8,128)(4,1)S(1)} %compare_bitcast_fusion), kind=kOutput, calls=%fused_computation | convolution fusion | flops 1519681536 | bytes 10251264 | tf_op jit(solution)/shard_map/sct,scd->std/dot_general | solution.py:131
  254.9 1.0 constant_dynamic-slice_fusion.1
  255.9 1.5 collective-permute-start.3
  257.4 22.5 %collective-permute-done.3 = bf16[512,1024]{1,0:T(8,128)(2,1)S(1)} collective-permute-done((bf16[512,1024]{1,0:T(8,128)(2,1)}, bf16[512,1024]{1,0:T(8,128)(2,1)S(1)}, u32[]{:S(2)}, u32[]{:S(2)}) %collective-permute-start.3) | collective-permute-done | bytes 1048608 | tf_op jit(solution)/shard_map/ppermute | solution.py:17
  279.9 0.6 broadcast_select_fusion.1
  280.4 1.5 maximum_bitcast_fusion
  281.9 42.2 %reduce-scatter.2.cloned.1.call-done = bf16[384,1024]{1,0:T(8,128)(2,1)} async-done(((bf16[3072,1024]{1,0:T(8,128)(2,1)}), bf16[384,1024]{1,0:T(8,128)(2,1)}) %reduce-scatter.2.cloned.1.call-update) | async-done | bytes 786448 | tf_op jit(solution)/shard_map/reduce_scatter | solution.py:133
  (46 shorter events, 0.4 us)
Async XLA Ops:
  7.2 2.0 copy-start.2
  7.2 121.8 %all-gather.7.cloned.1.call-start = ((), (), s32[]{:S(2)}) async-start(), calls=%async_computation.7 | async-start | bytes 3538944 | tf_op jit(solution)/shard_map/all_gather | solution.py:52
  9.1 1.2 copy-start.13
  71.0 31.8 %copy-start.11 = (f32[384,4]{0,1:T(4,128)S(1)}, f32[384,4]{0,1:T(4,128)}, u32[]{:S(2)}) copy-start(f32[384,4]{0,1:T(4,128)} %param.9) | copy-start | bytes 18436
  71.0 31.8 %copy-start.12 = (s32[384,4]{0,1:T(4,128)S(1)}, s32[384,4]{0,1:T(4,128)}, u32[]{:S(2)}) copy-start(s32[384,4]{0,1:T(4,128)} %param.8) | copy-start | bytes 18436
  71.0 30.2 %all-to-all-start.1 = ((bf16[8,128,512]{2,1,0:T(8,128)(2,1)}), bf16[8,128,512]{2,1,0:T(8,128)(2,1)S(1)}, u32[]{:S(2)}, u32[]{:S(2)}) async-start(bf16[8,128,512]{2,1,0:T(8,128)(2,1)} %get-tuple-element.11), calls=%async_computation.1 | async-start | bytes 2097152 | tf_op jit(solution)/shard_map/all_to_all | solution.py:68
  74.7 104.2 %all-gather.5.cloned.1.call-start = ((), (), s32[]{:S(2)}) async-start(), calls=%async_computation.6 | async-start | bytes 7077888 | tf_op jit(solution)/shard_map/all_gather | solution.py:75
  75.7 51.8 %copy-start.4 = (bf16[8,128,512]{2,1,0:T(8,128)(2,1)S(1)}, bf16[8,128,512]{2,1,0:T(8,128)(2,1)}, u32[]{:S(2)}) copy-start(bf16[8,128,512]{2,1,0:T(8,128)(2,1)} %all_to_all.27) | copy-start | bytes 3145732
  101.2 26.3 %collective-permute-start = (bf16[8,128,512]{2,1,0:T(8,128)(2,1)}, bf16[8,128,512]{2,1,0:T(8,128)(2,1)S(1)}, u32[]{:S(2)}, u32[]{:S(2)}) collective-permute-start(bf16[8,128,512]{2,1,0:T(8,128)(2,1)} %all_to_all.27), channel_id=1, source_target_pairs={{0,16},{16,0},{1,17},{17,1},{2,18},{18,2},{3,19},{19,3},{4,20},{20... | collective-permute-start | bytes 3145736 | tf_op jit(solution)/shard_map/ppermute | solution.py:17
  103.5 9.0 %all-to-all-start.3 = ((f32[8,1,384]{2,1,0:T(1,128)}), f32[8,1,384]{2,1,0:T(1,128)S(1)}, u32[]{:S(2)}, u32[]{:S(2)}) async-start(f32[8,1,384]{2,1,0:T(1,128)} %copy.53), calls=%async_computation.3 | async-start | bytes 24576 | tf_op jit(solution)/shard_map/all_to_all | solution.py:45
  112.6 36.1 %collective-permute-start.1 = (bf16[8,128,512]{2,1,0:T(8,128)(2,1)S(1)}, bf16[8,128,512]{2,1,0:T(8,128)(2,1)}, u32[]{:S(2)}, u32[]{:S(2)}) collective-permute-start(bf16[8,128,512]{2,1,0:T(8,128)(2,1)S(1)} %all-to-all-done.1), channel_id=1, source_target_pairs={{0,16},{16,0},{1,17},{17,1},{2,18},{18,2},{3,19},{19,3},{4,20},{20... | collective-permute-start | bytes 3145736 | tf_op jit(solution)/shard_map/ppermute | solution.py:17
  129.0 23.8 %copy-start.3 = (bf16[8,2,128,512]{3,2,1,0:T(8,128)(2,1)}, bf16[8,2,128,512]{3,2,1,0:T(8,128)(2,1)S(1)}, u32[]{:S(2)}) copy-start(bf16[8,2,128,512]{3,2,1,0:T(8,128)(2,1)S(1)} %pad_maximum_fusion) | copy-start | bytes 6291460
  132.9 42.1 %collective-permute-start.4 = (bf16[1920,512]{1,0:T(8,128)(2,1)S(1)}, bf16[1920,512]{1,0:T(8,128)(2,1)S(1)}, u32[]{:S(2)}, u32[]{:S(2)}) collective-permute-start(bf16[1920,512]{1,0:T(8,128)(2,1)S(1)} %bitcast.80), channel_id=1, source_target_pairs={{0,1},{1,0},{2,3},{3,2},{4,5},{5,4},{6,7},{7,6},{8,9},{9,8},{10,11... | collective-permute-start | bytes 5898248 | tf_op jit(solution)/shard_map/ppermute | solution.py:17
  150.3 31.9 %copy-start.9 = (bf16[4,2,128,512]{3,2,1,0:T(8,128)(2,1)}, bf16[4,2,128,512]{3,2,1,0:T(8,128)(2,1)S(1)}, u32[]{:S(2)}) copy-start(bf16[4,2,128,512]{3,2,1,0:T(8,128)(2,1)S(1)} %copy.56) | copy-start | bytes 3145732
  150.7 26.4 %copy-start = (bf16[8,2,128,512]{3,2,1,0:T(8,128)(2,1)}, bf16[8,2,128,512]{3,2,1,0:T(8,128)(2,1)S(1)}, u32[]{:S(2)}) copy-start(bf16[8,2,128,512]{3,2,1,0:T(8,128)(2,1)S(1)} %copy.51) | copy-start | bytes 6291460
  175.0 2.0 copy-start.5
  182.1 2.5 copy-start.8
  187.1 30.1 %all-to-all-start.2 = ((bf16[8,64,1024]{2,1,0:T(8,128)(2,1)}), bf16[8,64,1024]{2,1,0:T(8,128)(2,1)S(1)}, u32[]{:S(2)}, u32[]{:S(2)}) async-start(bf16[8,64,1024]{2,1,0:T(8,128)(2,1)} %dynamic-slice_convert_fusion), calls=%async_computation.2 | async-start | bytes 2097152 | tf_op jit(solution)/shard_map/all_to_all | solution.py:68
  190.6 133.5 %reduce-scatter.2.cloned.1.call-start = ((), (), s32[]{:S(2)}) async-start(), calls=%async_computation.5 | async-start | bytes 7077888 | tf_op jit(solution)/shard_map/reduce_scatter | solution.py:133
  197.5 5.9 %copy-start.10 = (bf16[4,2,128,512]{3,2,1,0:T(8,128)(2,1)S(1)}, bf16[4,2,128,512]{3,2,1,0:T(8,128)(2,1)}, u32[]{:S(2)}) copy-start(bf16[4,2,128,512]{3,2,1,0:T(8,128)(2,1)} %copy-done.9) | copy-start | bytes 3145732
  197.5 48.5 %collective-permute-start.5 = (bf16[960,512]{1,0:T(8,128)(2,1)}, bf16[960,512]{1,0:T(8,128)(2,1)}, u32[]{:S(2)}, u32[]{:S(2)}) collective-permute-start(bf16[960,512]{1,0:T(8,128)(2,1)} %multiply_convert_fusion.4), channel_id=1, source_target_pairs={{0,1},{1,0},{2,3},{3,2},{4,5},{5,4},{6,7},{7,6},{8,9},{9,8},{10,11... | collective-permute-start | bytes 2949128 | tf_op jit(solution)/shard_map/ppermute | solution.py:17
  202.2 1.3 copy-start.14
  217.2 5.3 %copy-start.1 = (f32[960,512]{1,0:T(8,128)S(1)}, f32[960,512]{1,0:T(8,128)}, u32[]{:S(2)}) copy-start(f32[960,512]{1,0:T(8,128)} %fusion.52) | copy-start | bytes 5898244
  217.2 5.3 %copy-start.6 = (bf16[1920,512]{1,0:T(8,128)(2,1)S(1)}, bf16[1920,512]{1,0:T(8,128)(2,1)}, u32[]{:S(2)}) copy-start(bf16[1920,512]{1,0:T(8,128)(2,1)} %copy-done.5) | copy-start | bytes 5898244
  217.2 5.3 %copy-start.7 = (f32[960,512]{1,0:T(8,128)S(1)}, f32[960,512]{1,0:T(8,128)}, u32[]{:S(2)}) copy-start(f32[960,512]{1,0:T(8,128)} %fusion.41) | copy-start | bytes 5898244
  217.2 5.3 %copy-start.15 = (f32[960,512]{1,0:T(8,128)S(1)}, f32[960,512]{1,0:T(8,128)}, u32[]{:S(2)}) copy-start(f32[960,512]{1,0:T(8,128)} %fusion.81) | copy-start | bytes 5898244
  217.2 24.7 %collective-permute-start.2 = (bf16[8,64,1024]{2,1,0:T(8,128)(2,1)S(1)}, bf16[8,64,1024]{2,1,0:T(8,128)(2,1)S(1)}, u32[]{:S(2)}, u32[]{:S(2)}) collective-permute-start(bf16[8,64,1024]{2,1,0:T(8,128)(2,1)S(1)} %all-to-all-done.2), channel_id=1, source_target_pairs={{0,16},{16,0},{1,17},{17,1},{2,18},{18,2},{3,19},{19,3},{4,20},{20... | collective-permute-start | bytes 3145736 | tf_op jit(solution)/shard_map/ppermute | solution.py:17
  225.1 23.4 %collective-permute-start.6 = (bf16[960,512]{1,0:T(8,128)(2,1)S(1)}, bf16[960,512]{1,0:T(8,128)(2,1)S(1)}, u32[]{:S(2)}, u32[]{:S(2)}) collective-permute-start(bf16[960,512]{1,0:T(8,128)(2,1)S(1)} %multiply_convert_fusion.3), channel_id=1, source_target_pairs={{0,1},{1,0},{2,3},{3,2},{4,5},{5,4},{6,7},{7,6},{8,9},{9,8},{10,11... | collective-permute-start | bytes 2949128 | tf_op jit(solution)/shard_map/ppermute | solution.py:17
  255.9 24.0 %collective-permute-start.3 = (bf16[512,1024]{1,0:T(8,128)(2,1)}, bf16[512,1024]{1,0:T(8,128)(2,1)S(1)}, u32[]{:S(2)}, u32[]{:S(2)}) collective-permute-start(bf16[512,1024]{1,0:T(8,128)(2,1)} %constant_dynamic-slice_fusion.1), channel_id=1, source_target_pairs={{0,1},{1,0},{2,3},{3,2},{4,5},{5,4},{6,7},{7,6},{8,9},{9,8},{10,11... | collective-permute-start | bytes 3145736 | tf_op jit(solution)/shard_map/ppermute | solution.py:17
Sparse Core Ops, SparseCore 0:
  10.4 63.2 all-gather.6
  101.4 63.6 all-gather.4
  255.0 69.1 reduce-scatter.1
